TPU v7x, 32 devices: a whole 2x2x4 slice. The times are simulated.
32 devices in a mesh: sp: 16 (over z, y, core), tp: 2 (over x).
Axes of the slice: x: 2, y: 2, z: 4, core: 2. Of those that a mesh axis runs over, the one named last changes fastest.
Arguments:
- residual: bfloat16 [2048, 2048], P(('sp', 'tp')), may hold values from -6 to 6
- q_small: bfloat16 [2048, 1024], P('sp', 'tp'), may hold values from -6 to 6
- k_small: bfloat16 [2048, 1024], P('sp', 'tp'), may hold values from -6 to 6
- v_small: bfloat16 [2048, 1024], P('sp', 'tp'), may hold values from -6 to 6
- q_large: bfloat16 [2048, 1024], P('sp', 'tp'), may hold values from -6 to 6
- k_large: bfloat16 [2048, 1024], P('sp', 'tp'), may hold values from -6 to 6
- v_large: bfloat16 [2048, 1024], P('sp', 'tp'), may hold values from -6 to 6
- forget_small: float32 [2048, 16], P('sp', 'tp'), may hold values from 0 to 20
- forget_large: float32 [2048, 8], P('sp', 'tp'), may hold values from 0 to 20
- w_out_small: bfloat16 [1024, 2048], P('tp'), may hold values from -0.125 to 0.125
- w_out_large: bfloat16 [1024, 2048], P('tp'), may hold values from -0.125 to 0.125
- norm_gain: float32 [2048], replicated, may hold values from 0.1 to 1.9
- w_gate: bfloat16 [2048, 4096], P('sp', 'tp'), may hold values from -0.125 to 0.125
- w_up: bfloat16 [2048, 4096], P('sp', 'tp'), may hold values from -0.125 to 0.125
- conv_gate: float32 [3, 4096], P(None, 'tp'), may hold values from -3 to 3
- conv_up: float32 [3, 4096], P(None, 'tp'), may hold values from -3 to 3
- w_down: bfloat16 [4096, 2048], P('tp', 'sp'), may hold values from -0.09375 to 0.09375
Outputs:
- mixed: bfloat16 [2048, 2048], P(('sp', 'tp'))
All inputs are finite; a program needn't handle non-finite values.
Results may differ from a plain program's by a relative error of at most 0.015.
Values may be sent and summed in bfloat16 or wider, within the bound.
A program may use at most 64 MiB of HBM per device.

v0:
```python
import jax
import jax.numpy as jnp
from jax import lax
from jax.sharding import PartitionSpec as P

EPS = 1e-06
NEG = -1e30


def from_behind(block, axis, distance):
    devices = range(lax.axis_size(axis))
    route = [(i - distance, i) for i in devices if i - distance in devices]
    return lax.ppermute(block, axis, route)


def globalize(part, rows):
    heads = part.shape[1]
    blocks = part.reshape(-1, rows, heads)
    totals = blocks[:, -1, :]
    before = jnp.cumsum(totals, axis=0) - totals
    return (blocks + before[:, None, :]).reshape(part.shape)


def attend(carry, keys, values, queries, cum_own, cum_every, qpos):
    top, denom, accum = carry
    count = keys.shape[0]
    heads = queries.shape[1]
    size = queries.shape[2]
    keys = keys.reshape(count, heads, size)
    values = values.reshape(count, heads, size)
    kpos = jnp.arange(count, dtype=jnp.int32)
    scores = jnp.einsum(
        "qhd,khd->qhk", queries, keys, preferred_element_type=jnp.float32
    ) * size ** (-0.5)
    scores = scores + cum_own[:, :, None] - cum_every.T[None, :, :]
    keep = (kpos[None, :] <= qpos[:, None])[:, None, :]
    scores = jnp.where(keep, scores, NEG)
    new_top = jnp.maximum(top, jnp.max(scores, axis=-1))
    weights = jnp.where(keep, jnp.exp(scores - new_top[:, :, None]), 0.0)
    denom = jnp.sum(weights, axis=-1)
    accum = jnp.einsum(
        "qhk,khd->qhd", weights.astype(jnp.bfloat16), values, preferred_element_type=jnp.float32
    )
    return (new_top, denom, accum)


def finish(carry):
    top, denom, accum = carry
    attended = accum / denom[:, :, None]
    normed = attended * lax.rsqrt(jnp.mean(attended * attended, axis=-1, keepdims=True) + EPS)
    return normed.astype(jnp.bfloat16).reshape(attended.shape[0], -1)


def empty_carry(rows, heads, size):
    return (
        jnp.full((rows, heads), NEG, jnp.float32),
        jnp.zeros((rows, heads), jnp.float32),
        jnp.zeros((rows, heads, size), jnp.float32),
    )


def body(
    residual,
    q_small,
    k_small,
    v_small,
    q_large,
    k_large,
    v_large,
    forget_small,
    forget_large,
    w_out_small,
    w_out_large,
    norm_gain,
    w_gate,
    w_up,
    conv_gate,
    conv_up,
    w_down,
):
    rows = q_small.shape[0]
    offset = lax.axis_index("sp") * rows
    qpos = offset + jnp.arange(rows, dtype=jnp.int32)
    gathered = (
        lax.all_gather(w_gate, "sp", axis=0, tiled=True),
        lax.all_gather(w_up, "sp", axis=0, tiled=True),
        lax.all_gather(w_down, "sp", axis=1, tiled=True),
    )
    local_small = jnp.cumsum(jax.nn.log_sigmoid(forget_small), axis=0)
    local_large = jnp.cumsum(jax.nn.log_sigmoid(forget_large), axis=0)
    part_small, part_large = (
        lax.all_gather(local_small, "sp", axis=0, tiled=True),
        lax.all_gather(local_large, "sp", axis=0, tiled=True),
    )
    every_small = globalize(part_small, rows)
    every_large = globalize(part_large, rows)
    cum_small = lax.dynamic_slice_in_dim(every_small, offset, rows, 0)
    cum_large = lax.dynamic_slice_in_dim(every_large, offset, rows, 0)
    heads_small = forget_small.shape[1]
    heads_large = forget_large.shape[1]
    queries_small = q_small.reshape(rows, heads_small, -1)
    queries_large = q_large.reshape(rows, heads_large, -1)
    start_carry = (
        empty_carry(rows, heads_small, queries_small.shape[2]),
        empty_carry(rows, heads_large, queries_large.shape[2]),
    )
    keys_s = lax.all_gather(k_small, "sp", axis=0, tiled=True)
    values_s = lax.all_gather(v_small, "sp", axis=0, tiled=True)
    keys_l = lax.all_gather(k_large, "sp", axis=0, tiled=True)
    values_l = lax.all_gather(v_large, "sp", axis=0, tiled=True)
    small = attend(start_carry[0], keys_s, values_s, queries_small, cum_small, every_small, qpos)
    large = attend(start_carry[1], keys_l, values_l, queries_large, cum_large, every_large, qpos)
    normed_small = finish(small)
    normed_large = finish(large)
    first_part = jnp.dot(normed_small, w_out_small, preferred_element_type=jnp.float32)
    projected = lax.psum_scatter(
        (
            first_part + jnp.dot(normed_large, w_out_large, preferred_element_type=jnp.float32)
        ).astype(jnp.bfloat16),
        "tp",
        scatter_dimension=0,
        tiled=True,
    ).astype(jnp.float32)
    first = residual.astype(jnp.float32) + projected
    normal = (
        first * lax.rsqrt(jnp.mean(first * first, axis=-1, keepdims=True) + EPS) * norm_gain
    ).astype(jnp.bfloat16)
    gate_full, up_full, down_full = gathered
    piece = lax.all_gather(normal, "tp", axis=0, tiled=True)
    gate_part = jnp.dot(piece, gate_full, preferred_element_type=jnp.float32).astype(jnp.bfloat16)
    up_part = jnp.dot(piece, up_full, preferred_element_type=jnp.float32).astype(jnp.bfloat16)
    both = jnp.concatenate([gate_part, up_part], axis=1)
    width = both.shape[0]
    rim = from_behind(both[width - 2 :], "sp", 1)
    extended = jnp.concatenate([rim, both], axis=0).astype(jnp.float32)
    taps = jnp.concatenate([conv_gate, conv_up], axis=1)
    conv = (
        taps[0] * extended[0:width]
        + taps[1] * extended[1 : width + 1]
        + taps[2] * extended[2 : width + 2]
    )
    half = gate_full.shape[1]
    hidden = (jax.nn.silu(conv[:, :half]) * conv[:, half:]).astype(jnp.bfloat16)
    mixed = first + lax.psum_scatter(
        jnp.dot(hidden, down_full, preferred_element_type=jnp.float32).astype(jnp.bfloat16),
        "tp",
        scatter_dimension=0,
        tiled=True,
    ).astype(jnp.float32)
    return mixed.astype(jnp.bfloat16)


def solution(mesh):
    placed = (
        P(("sp", "tp"), None),
        P("sp", "tp"),
        P("sp", "tp"),
        P("sp", "tp"),
        P("sp", "tp"),
        P("sp", "tp"),
        P("sp", "tp"),
        P("sp", "tp"),
        P("sp", "tp"),
        P("tp", None),
        P("tp", None),
        P(),
        P("sp", "tp"),
        P("sp", "tp"),
        P(None, "tp"),
        P(None, "tp"),
        P("tp", "sp"),
    )
    return jax.shard_map(
        body, mesh=mesh, in_specs=placed, out_specs=P(("sp", "tp"), None), check_vma=False
    )
```

profile of v0, /device:TPU:0, one launch (start us, length us, event | category | flops | bytes accessed | tf_op | source)
XLA Modules:
  0.0 472.0 jit_solution(16428870450614130786)
XLA Ops:
  8.1 1.7 copy.44
  11.4 27.1 %all_gather.34 = f32[2048,4]{1,0:T(8,128)S(1)} all-gather(f32[128,4]{1,0:T(8,128)S(1)} %reduce_window_sum.46), channel_id=1, replica_groups=mesh['sp'=16,'tp'=2] {'sp'}, dimensions={0}, use_global_device_ids=true | all-gather | bytes 34816 | tf_op jit(solution)/shard_map/all_gather | solution.py:93
  38.8 24.5 %all_gather.31 = f32[2048,8]{1,0:T(8,128)S(1)} all-gather(f32[128,8]{1,0:T(8,128)S(1)} %reduce_window_sum.44), channel_id=1, replica_groups=mesh['sp'=16,'tp'=2] {'sp'}, dimensions={0}, use_global_device_ids=true | all-gather | bytes 69632 | tf_op jit(solution)/shard_map/all_gather | solution.py:92
  63.4 1.1 bitcast_add_fusion.3
  65.7 1.6 copy.41
  67.7 4.0 copy.52
  71.7 31.4 %all-gather.8.cloned.1.call-done = bf16[2048,512]{1,0:T(8,128)(2,1)} async-done(((bf16[128,512]{1,0:T(8,128)(2,1)}), bf16[2048,512]{1,0:T(8,128)(2,1)}) %all-gather.8.cloned.1.call-update) | async-done | bytes 2097168 | tf_op jit(solution)/shard_map/all_gather | solution.py:107
  103.0 4.0 copy.35
  107.0 38.0 %all-gather.12.cloned.1.call-done = bf16[2048,512]{0,1:T(8,128)(2,1)} async-done(((bf16[128,512]{0,1:T(8,128)(2,1)}), bf16[2048,512]{0,1:T(8,128)(2,1)}) %all-gather.12.cloned.1.call-update) | async-done | bytes 2097168 | tf_op jit(solution)/shard_map/all_gather | solution.py:109
  145.0 3.7 fusion.47
  150.3 1.2 multiply_reduce_fusion.1
  151.9 3.4 fusion.4
  155.3 3.2 copy-done.2
  158.5 3.1 fusion.2
  161.6 26.0 %all-gather.10.cloned.1.call-done = bf16[2048,512]{1,0:T(8,128)(2,1)} async-done(((bf16[128,512]{1,0:T(8,128)(2,1)}), bf16[2048,512]{1,0:T(8,128)(2,1)}) %all-gather.10.cloned.1.call-update) | async-done | bytes 2097168 | tf_op jit(solution)/shard_map/all_gather | solution.py:108
  187.6 3.9 copy.42
  191.5 6.6 %multiply_reduce_fusion.2 = (f32[128,8]{0,1:T(8,128)S(1)}, f32[128,8,64]{0,2,1:T(8,128)S(1)}) fusion(f32[128,8]{0,1:T(8,128)S(1)} %fusion.2, bf16[2048,8,64]{0,2,1:T(8,128)(2,1)} %bitcast.82, f32[8,2048,128]{2,1,0:T(8,128)} %copy-done.2, f32[128,8]{0,1:T(8,128)S(1)} %broadcast_maximum_fusion, f32[8,2048]{1,0:T(8,128)S(1)} %copy.41, f32[128,8]{0,1:T(8,128)S(1)} %copy.40, ...), kind=kOutput, calls=%fused_computation.49 | convolution fusion | flops 283311104 | bytes 11091968 | tf_op jit(solution)/shard_map/qhk,khd->qhd/dot_general | solution.py:41
  199.7 1.3 fusion.12
  203.2 11.3 %reduce-scatter.3.cloned.1.call-done = bf16[64,2048]{1,0:T(8,128)(2,1)} async-done(((bf16[128,2048]{1,0:T(8,128)(2,1)}), bf16[64,2048]{1,0:T(8,128)(2,1)}) %reduce-scatter.3.cloned.1.call-update) | async-done | bytes 262160 | tf_op jit(solution)/shard_map/reduce_scatter | solution.py:116
  214.6 1.1 multiply_reduce_fusion
  215.7 1.1 multiply_convert_fusion
  216.8 8.7 %all_gather.36 = bf16[128,2048]{1,0:T(8,128)(2,1)S(1)} all-gather(bf16[64,2048]{1,0:T(8,128)(2,1)S(1)} %multiply_convert_fusion), channel_id=1, replica_groups=mesh['sp'=16,'tp'=2] {'tp'}, dimensions={0}, use_global_device_ids=true | all-gather | bytes 786432 | tf_op jit(solution)/shard_map/all_gather | solution.py:129
  225.5 65.4 %all-gather.18.cloned.1.call-done = bf16[2048,2048]{1,0:T(8,128)(2,1)} async-done(((bf16[128,2048]{1,0:T(8,128)(2,1)}), bf16[2048,2048]{1,0:T(8,128)(2,1)}) %all-gather.18.cloned.1.call-update) | async-done | bytes 8388624 | tf_op jit(solution)/shard_map/all_gather | solution.py:86
  290.9 4.6 convolution_convert_fusion.1
  295.6 70.4 %all-gather.16.cloned.1.call-done = bf16[2048,2048]{1,0:T(8,128)(2,1)} async-done(((bf16[128,2048]{1,0:T(8,128)(2,1)}), bf16[2048,2048]{1,0:T(8,128)(2,1)}) %all-gather.16.cloned.1.call-update) | async-done | bytes 8388624 | tf_op jit(solution)/shard_map/all_gather | solution.py:85
  366.0 4.6 convolution_convert_fusion.2
  370.7 2.2 collective-permute-start
  373.9 2.0 fusion.15
  375.9 68.5 %all-gather.20.cloned.1.call-done = bf16[2048,2048]{1,0:T(8,128)(2,1)} async-done(((bf16[2048,128]{1,0:T(8,128)(2,1)}), bf16[2048,2048]{1,0:T(8,128)(2,1)}) %all-gather.20.cloned.1.call-update) | async-done | bytes 8388624 | tf_op jit(solution)/shard_map/all_gather | solution.py:87
  444.5 6.3 %convolution_convert_fusion = bf16[128,2048]{1,0:T(8,128)(2,1)} fusion(bf16[2048,2048]{1,0:T(8,128)(2,1)} %all-gather.20.cloned.1.call-done, f32[128,4096]{1,0:T(8,128)} %fusion.15), kind=kOutput, calls=%fused_computation.16 | convolution fusion | flops 1075576832 | bytes 11010048 | tf_op jit(solution)/shard_map/dot_general | solution.py:145
  450.8 13.0 %reduce-scatter.5.cloned.1.call-done = bf16[64,2048]{1,0:T(8,128)(2,1)} async-done(((bf16[128,2048]{1,0:T(8,128)(2,1)}), bf16[64,2048]{1,0:T(8,128)(2,1)}) %reduce-scatter.5.cloned.1.call-update) | async-done | bytes 262160 | tf_op jit(solution)/shard_map/reduce_scatter | solution.py:144
  463.8 1.7 add_convert_fusion
  (78 shorter events, 12.0 us)
Async XLA Ops:
  6.5 191.7 %copy-start = (bf16[512,2048]{1,0:T(8,128)(2,1)S(1)}, bf16[512,2048]{1,0:T(8,128)(2,1)}, u32[]{:S(2)}) copy-start(bf16[512,2048]{1,0:T(8,128)(2,1)} %param.26) | copy-start | bytes 6291460
  6.5 32.0 %copy-start.12 = (f32[128,8]{0,1:T(8,128)S(1)}, f32[128,8]{0,1:T(8,128)}, u32[]{:S(2)}) copy-start(f32[128,8]{0,1:T(8,128)} %param.24) | copy-start | bytes 12292
  6.5 61.1 %all-gather.14.cloned.1.call-start = ((), (), s32[]{:S(2)}) async-start(), calls=%async_computation.5 | async-start | bytes 2228224 | tf_op jit(solution)/shard_map/all_gather | solution.py:110
  7.3 95.8 %all-gather.8.cloned.1.call-start = ((), (), s32[]{:S(2)}) async-start(), calls=%async_computation.2 | async-start | bytes 2228224 | tf_op jit(solution)/shard_map/all_gather | solution.py:107
  8.0 137.0 %all-gather.12.cloned.1.call-start = ((), (), s32[]{:S(2)}) async-start(), calls=%async_computation.4 | async-start | bytes 2228224 | tf_op jit(solution)/shard_map/all_gather | solution.py:109
  9.7 177.8 %all-gather.10.cloned.1.call-start = ((), (), s32[]{:S(2)}) async-start(), calls=%async_computation.3 | async-start | bytes 2228224 | tf_op jit(solution)/shard_map/all_gather | solution.py:108
  10.3 204.2 %reduce-scatter.3.cloned.1.call-start = ((), (), s32[]{:S(2)}) async-start(), calls=%async_computation.6 | async-start | bytes 786432 | tf_op jit(solution)/shard_map/reduce_scatter | solution.py:116
  38.4 28.9 %copy-start.8 = (bf16[128,512]{1,0:T(8,128)(2,1)S(1)}, bf16[128,512]{1,0:T(8,128)(2,1)}, u32[]{:S(2)}) copy-start(bf16[128,512]{1,0:T(8,128)(2,1)} %param.18) | copy-start | bytes 393220
  67.6 77.4 %copy-start.13 = (bf16[128,512]{1,0:T(8,128)(2,1)S(1)}, bf16[128,512]{1,0:T(8,128)(2,1)}, u32[]{:S(2)}) copy-start(bf16[128,512]{1,0:T(8,128)(2,1)} %param.21) | copy-start | bytes 393220
  148.7 1.6 copy-start.7
  150.3 1.6 copy-start.6
  155.2 3.2 copy-start.2
  198.1 1.6 copy-start.5
  198.2 5.0 %copy-start.9 = (f32[3,2048]{1,0:T(4,128)S(1)}, f32[3,2048]{1,0:T(4,128)}, u32[]{:S(2)}) copy-start(f32[3,2048]{1,0:T(4,128)} %param.31) | copy-start | bytes 73732
  198.2 5.0 %copy-start.10 = (f32[3,2048]{1,0:T(4,128)S(1)}, f32[3,2048]{1,0:T(4,128)}, u32[]{:S(2)}) copy-start(f32[3,2048]{1,0:T(4,128)} %param.32) | copy-start | bytes 73732
  198.3 16.3 %copy-start.3 = (bf16[64,2048]{1,0:T(8,128)(2,1)S(1)}, bf16[64,2048]{1,0:T(8,128)(2,1)}, u32[]{:S(2)}) copy-start(bf16[64,2048]{1,0:T(8,128)(2,1)} %param.17) | copy-start | bytes 786436
  198.3 17.5 %copy-start.11 = (f32[2048]{0:T(1024)S(1)}, f32[2048]{0:T(1024)}, u32[]{:S(2)}) copy-start(f32[2048]{0:T(1024)} %param.28) | copy-start | bytes 24580
  201.1 89.8 %all-gather.18.cloned.1.call-start = ((), (), s32[]{:S(2)}) async-start(), calls=%async_computation.8 | async-start | bytes 8912896 | tf_op jit(solution)/shard_map/all_gather | solution.py:86
  201.6 164.3 %all-gather.16.cloned.1.call-start = ((), (), s32[]{:S(2)}) async-start(), calls=%async_computation.7 | async-start | bytes 8912896 | tf_op jit(solution)/shard_map/all_gather | solution.py:85
  202.4 242.1 %all-gather.20.cloned.1.call-start = ((), (), s32[]{:S(2)}) async-start(), calls=%async_computation.9 | async-start | bytes 8912896 | tf_op jit(solution)/shard_map/all_gather | solution.py:87
  203.1 260.6 %reduce-scatter.5.cloned.1.call-start = ((), (), s32[]{:S(2)}) async-start(), calls=%async_computation.10 | async-start | bytes 786432 | tf_op jit(solution)/shard_map/reduce_scatter | solution.py:144
  370.7 3.0 collective-permute-start
  375.9 87.8 %copy-start.4 = (bf16[64,2048]{1,0:T(8,128)(2,1)S(1)}, bf16[64,2048]{1,0:T(8,128)(2,1)}, u32[]{:S(2)}) copy-start(bf16[64,2048]{1,0:T(8,128)(2,1)} %reduce-scatter.3.cloned.1.call-done) | copy-start | bytes 786436
  444.5 21.0 %copy-start.1 = (bf16[512,2048]{1,0:T(8,128)(2,1)S(1)}, bf16[512,2048]{1,0:T(8,128)(2,1)}, u32[]{:S(2)}) copy-start(bf16[512,2048]{1,0:T(8,128)(2,1)} %param.26) | copy-start | bytes 6291460
Sparse Core Ops, SparseCore 0:
  9.5 49.7 all-gather.13
  61.4 41.5 all-gather.7
  105.2 39.7 all-gather.11
  147.0 40.5 all-gather.9
  201.2 13.3 reduce-scatter.2
  216.6 74.2 all-gather.17
  293.1 72.8 all-gather.15
  368.1 76.2 all-gather.19
  450.9 12.7 reduce-scatter.4
where the time goes:
time: 473 us; the launch traced here: 472 us
  waiting for transfers between devices  329 us (70%)
  blocking collectives  60.3 us (13%)
  matrix products  32.2 us (7%)
  local copies, waits for them, and re-layouts  22.4 us (5%)
  between operations  13.5 us (3%)
  other arithmetic  12.6 us (3%)
    all_gather x1, waiting for transfers between devices, body(): lax.all_gather(w_gate, 'sp', axis=0, tiled=True)  70.4 us
    all_gather x1, waiting for transfers between devices, body(): lax.all_gather(w_down, 'sp', axis=1, tiled=True)  68.5 us
    all_gather x1, waiting for transfers between devices, body(): lax.all_gather(w_up, 'sp', axis=0, tiled=True)  65.4 us
    all_gather x1, waiting for transfers between devices, body(): keys_l = lax.all_gather(k_large, 'sp', axis=0, tiled=True)  38 us
    all_gather x1, waiting for transfers between devices, body(): keys_s = lax.all_gather(k_small, 'sp', axis=0, tiled=True)  31.4 us
    all_gather x1, blocking collectives, body(): lax.all_gather(local_large, 'sp', axis=0, tiled=True)  27.1 us
    all_gather x1, waiting for transfers between devices, body(): values_s = lax.all_gather(v_small, 'sp', axis=0, tiled=True)  26 us
    all_gather x1, blocking collectives, body(): lax.all_gather(local_small, 'sp', axis=0, tiled=True)  24.5 us
  transfers between devices with their start and end apart: 10, of which 9 were waited for; matrix products, arithmetic and copies ran while one was open for 9% of the time, Pallas kernels for 0%

commit v1 on v0

--- a/solution.py
+++ b/solution.py
@@ -105,7 +105,12 @@
         empty_carry(rows, heads_large, queries_large.shape[2]),
     )
     keys_s = lax.all_gather(k_small, "sp", axis=0, tiled=True)
-    values_s = lax.all_gather(v_small, "sp", axis=0, tiled=True)
+    ring = [v_small]
+    for hop in range(15):
+        ring.append(lax.ppermute(ring[-1], "sp", [(dev, (dev + 1) % 16) for dev in range(16)]))
+    values_s = jnp.roll(
+        jnp.concatenate(ring[::-1], axis=0), (lax.axis_index("sp") + 1) * ring[0].shape[0], axis=0
+    )
     keys_l = lax.all_gather(k_large, "sp", axis=0, tiled=True)
     values_l = lax.all_gather(v_large, "sp", axis=0, tiled=True)
     small = attend(start_carry[0], keys_s, values_s, queries_small, cum_small, every_small, qpos)

time: 473 us -> 492 us (1.040)
  local copies, waits for them, and re-layouts: 22.4 us -> 46.9 us
  waiting for transfers between devices: 329 us -> 323 us
    ppermute x0 -> x15, waiting for transfers between devices: none -> 87.5 us  [body(): lax.ppermute(ring[-1], 'sp', [(dev, (dev + 1) % 16) for dev in range(16)])]
    all_gather x1, waiting for transfers between devices: 38 us -> 0.01 us  [body(): keys_l = lax.all_gather(k_large, 'sp', axis=0, tiled=True)]
    all_gather x1, waiting for transfers between devices: 31.4 us -> 0.01 us  [body(): keys_s = lax.all_gather(k_small, 'sp', axis=0, tiled=True)]
    all_gather x1 -> x0, waiting for transfers between devices: 26 us -> none  [body(): values_s = lax.all_gather(v_small, 'sp', axis=0, tiled=True)]
    unnamed x31 -> x114, local copies, waits for them, and re-layouts: 7.27 us -> 27.5 us
    dynamic_slice x0 -> x2, local copies, waits for them, and re-layouts: none -> 5.54 us  [body(): jnp.roll(jnp.concatenate(ring[::-1], axis=0), (lax.axis_index('sp') + 1)...]
  transfers between devices with their start and end apart: 10 -> 24, of which waited for: 9 -> 18; matrix products, arithmetic and copies ran while one was open for 9% -> 14% of each run, Pallas kernels for 0% -> 0%
where the time goes in v1:
time: 492 us; the launch traced here: 491 us
  waiting for transfers between devices  323 us (66%)
  blocking collectives  57.5 us (12%)
  local copies, waits for them, and re-layouts  46.9 us (10%)
  matrix products  31.8 us (6%)
  other arithmetic  14.2 us (3%)
  between operations  14.2 us (3%)
    ppermute x15, waiting for transfers between devices, body(): lax.ppermute(ring[-1], 'sp', [(dev, (dev + 1) % 16) for dev in range(16)])  87.5 us
    all_gather x1, waiting for transfers between devices, body(): lax.all_gather(w_gate, 'sp', axis=0, tiled=True)  70.3 us
    all_gather x1, waiting for transfers between devices, body(): lax.all_gather(w_down, 'sp', axis=1, tiled=True)  68.6 us
    all_gather x1, waiting for transfers between devices, body(): lax.all_gather(w_up, 'sp', axis=0, tiled=True)  65.3 us
    unnamed x114, local copies, waits for them, and re-layouts  27.5 us
    all_gather x1, blocking collectives, body(): lax.all_gather(local_large, 'sp', axis=0, tiled=True)  25 us
    all_gather x1, blocking collectives, body(): lax.all_gather(local_small, 'sp', axis=0, tiled=True)  23.7 us
    reduce_scatter x1, waiting for transfers between devices, body(): lax.psum_scatter((first_part + jnp.dot(normed_large, w_out_large, preferr...  14.8 us
  transfers between devices with their start and end apart: 24, of which 18 were waited for; matrix products, arithmetic and copies ran while one was open for 14% of the time, Pallas kernels for 0%

profile of v1, /device:TPU:0, one launch (start us, length us, event | category | flops | bytes accessed | tf_op | source)
XLA Modules:
  0.0 490.9 jit_solution(10963269098566777868)
XLA Ops:
  9.6 7.8 %collective-permute-done = bf16[128,512]{1,0:T(8,128)(2,1)S(1)} collective-permute-done((bf16[128,512]{1,0:T(8,128)(2,1)}, bf16[128,512]{1,0:T(8,128)(2,1)S(1)}, u32[]{:S(2)}, u32[]{:S(2)}) %collective-permute-start) | collective-permute-done | bytes 131104 | tf_op jit(solution)/shard_map/ppermute | solution.py:110
  18.1 7.2 %collective-permute-done.1 = bf16[128,512]{1,0:T(8,128)(2,1)S(1)} collective-permute-done((bf16[128,512]{1,0:T(8,128)(2,1)S(1)}, bf16[128,512]{1,0:T(8,128)(2,1)S(1)}, u32[]{:S(2)}, u32[]{:S(2)}) %collective-permute-start.1) | collective-permute-done | bytes 131104 | tf_op jit(solution)/shard_map/ppermute | solution.py:110
  26.0 7.4 %collective-permute-done.2 = bf16[128,512]{1,0:T(8,128)(2,1)S(1)} collective-permute-done((bf16[128,512]{1,0:T(8,128)(2,1)S(1)}, bf16[128,512]{1,0:T(8,128)(2,1)S(1)}, u32[]{:S(2)}, u32[]{:S(2)}) %collective-permute-start.2) | collective-permute-done | bytes 131104 | tf_op jit(solution)/shard_map/ppermute | solution.py:110
  34.0 7.2 %collective-permute-done.3 = bf16[128,512]{1,0:T(8,128)(2,1)S(1)} collective-permute-done((bf16[128,512]{1,0:T(8,128)(2,1)S(1)}, bf16[128,512]{1,0:T(8,128)(2,1)S(1)}, u32[]{:S(2)}, u32[]{:S(2)}) %collective-permute-start.3) | collective-permute-done | bytes 131104 | tf_op jit(solution)/shard_map/ppermute | solution.py:110
  41.9 7.9 %collective-permute-done.4 = bf16[128,512]{1,0:T(8,128)(2,1)S(1)} collective-permute-done((bf16[128,512]{1,0:T(8,128)(2,1)S(1)}, bf16[128,512]{1,0:T(8,128)(2,1)S(1)}, u32[]{:S(2)}, u32[]{:S(2)}) %collective-permute-start.4) | collective-permute-done | bytes 131104 | tf_op jit(solution)/shard_map/ppermute | solution.py:110
  50.4 7.1 %collective-permute-done.5 = bf16[128,512]{1,0:T(8,128)(2,1)S(1)} collective-permute-done((bf16[128,512]{1,0:T(8,128)(2,1)S(1)}, bf16[128,512]{1,0:T(8,128)(2,1)S(1)}, u32[]{:S(2)}, u32[]{:S(2)}) %collective-permute-start.5) | collective-permute-done | bytes 131104 | tf_op jit(solution)/shard_map/ppermute | solution.py:110
  58.1 7.1 %collective-permute-done.6 = bf16[128,512]{1,0:T(8,128)(2,1)S(1)} collective-permute-done((bf16[128,512]{1,0:T(8,128)(2,1)S(1)}, bf16[128,512]{1,0:T(8,128)(2,1)S(1)}, u32[]{:S(2)}, u32[]{:S(2)}) %collective-permute-start.6) | collective-permute-done | bytes 131104 | tf_op jit(solution)/shard_map/ppermute | solution.py:110
  65.9 7.2 %collective-permute-done.7 = bf16[128,512]{1,0:T(8,128)(2,1)S(1)} collective-permute-done((bf16[128,512]{1,0:T(8,128)(2,1)S(1)}, bf16[128,512]{1,0:T(8,128)(2,1)S(1)}, u32[]{:S(2)}, u32[]{:S(2)}) %collective-permute-start.7) | collective-permute-done | bytes 131104 | tf_op jit(solution)/shard_map/ppermute | solution.py:110
  73.2 7.0 %collective-permute-done.8 = bf16[128,512]{1,0:T(8,128)(2,1)S(1)} collective-permute-done((bf16[128,512]{1,0:T(8,128)(2,1)S(1)}, bf16[128,512]{1,0:T(8,128)(2,1)S(1)}, u32[]{:S(2)}, u32[]{:S(2)}) %collective-permute-start.8) | collective-permute-done | bytes 131104 | tf_op jit(solution)/shard_map/ppermute | solution.py:110
  80.4 7.1 %collective-permute-done.9 = bf16[128,512]{1,0:T(8,128)(2,1)S(1)} collective-permute-done((bf16[128,512]{1,0:T(8,128)(2,1)S(1)}, bf16[128,512]{1,0:T(8,128)(2,1)S(1)}, u32[]{:S(2)}, u32[]{:S(2)}) %collective-permute-start.9) | collective-permute-done | bytes 131104 | tf_op jit(solution)/shard_map/ppermute | solution.py:110
  88.5 23.7 %all_gather.28 = f32[2048,8]{1,0:T(8,128)S(1)} all-gather(f32[128,8]{1,0:T(8,128)S(1)} %reduce_window_sum.44), channel_id=1, replica_groups=mesh['sp'=16,'tp'=2] {'sp'}, dimensions={0}, use_global_device_ids=true | all-gather | bytes 69632 | tf_op jit(solution)/shard_map/all_gather | solution.py:92
  112.7 8.1 %collective-permute-done.11 = bf16[128,512]{1,0:T(8,128)(2,1)} collective-permute-done((bf16[128,512]{1,0:T(8,128)(2,1)S(1)}, bf16[128,512]{1,0:T(8,128)(2,1)}, u32[]{:S(2)}, u32[]{:S(2)}) %collective-permute-start.11) | collective-permute-done | bytes 131104 | tf_op jit(solution)/shard_map/ppermute | solution.py:110
  123.2 25.0 %all_gather.30 = f32[2048,4]{1,0:T(8,128)S(1)} all-gather(f32[128,4]{1,0:T(8,128)} %reduce_window_sum.46), channel_id=1, replica_groups=mesh['sp'=16,'tp'=2] {'sp'}, dimensions={0}, use_global_device_ids=true | all-gather | bytes 34816 | tf_op jit(solution)/shard_map/all_gather | solution.py:93
  149.1 6.4 %collective-permute-done.13 = bf16[128,512]{1,0:T(8,128)(2,1)} collective-permute-done((bf16[128,512]{1,0:T(8,128)(2,1)}, bf16[128,512]{1,0:T(8,128)(2,1)}, u32[]{:S(2)}, u32[]{:S(2)}) %collective-permute-start.13) | collective-permute-done | bytes 131104 | tf_op jit(solution)/shard_map/ppermute | solution.py:110
  183.0 4.1 copy.35
  187.1 4.0 copy.36
  191.1 3.8 fusion.47
  195.0 3.4 fusion.4
  198.5 3.1 fusion.2
  201.6 3.3 multiply_reduce_fusion.2
  205.7 4.0 copy.52
  209.7 3.9 multiply_reduce_fusion.1
  218.5 14.8 %reduce-scatter.3.cloned.1.call-done = bf16[64,2048]{1,0:T(8,128)(2,1)} async-done(((bf16[128,2048]{1,0:T(8,128)(2,1)}), bf16[64,2048]{1,0:T(8,128)(2,1)}) %reduce-scatter.3.cloned.1.call-update) | async-done | bytes 262160 | tf_op jit(solution)/shard_map/reduce_scatter | solution.py:121
  235.6 8.8 %all_gather.32 = bf16[128,2048]{1,0:T(8,128)(2,1)S(1)} all-gather(bf16[64,2048]{1,0:T(8,128)(2,1)S(1)} %multiply_convert_fusion), channel_id=1, replica_groups=mesh['sp'=16,'tp'=2] {'tp'}, dimensions={0}, use_global_device_ids=true | all-gather | bytes 786432 | tf_op jit(solution)/shard_map/all_gather | solution.py:134
  244.3 65.3 %all-gather.15.cloned.1.call-done = bf16[2048,2048]{1,0:T(8,128)(2,1)} async-done(((bf16[128,2048]{1,0:T(8,128)(2,1)}), bf16[2048,2048]{1,0:T(8,128)(2,1)}) %all-gather.15.cloned.1.call-update) | async-done | bytes 8388624 | tf_op jit(solution)/shard_map/all_gather | solution.py:86
  309.7 4.6 convolution_convert_fusion.1
  314.3 70.3 %all-gather.13.cloned.1.call-done = bf16[2048,2048]{1,0:T(8,128)(2,1)} async-done(((bf16[128,2048]{1,0:T(8,128)(2,1)}), bf16[2048,2048]{1,0:T(8,128)(2,1)}) %all-gather.13.cloned.1.call-update) | async-done | bytes 8388624 | tf_op jit(solution)/shard_map/all_gather | solution.py:85
  384.6 4.6 convolution_convert_fusion.2
  389.3 2.2 collective-permute-start.15
  394.5 68.6 %all-gather.17.cloned.1.call-done = bf16[2048,2048]{1,0:T(8,128)(2,1)} async-done(((bf16[2048,128]{1,0:T(8,128)(2,1)}), bf16[2048,2048]{1,0:T(8,128)(2,1)}) %all-gather.17.cloned.1.call-update) | async-done | bytes 8388624 | tf_op jit(solution)/shard_map/all_gather | solution.py:87
  463.1 6.3 %convolution_convert_fusion = bf16[128,2048]{1,0:T(8,128)(2,1)} fusion(bf16[2048,2048]{1,0:T(8,128)(2,1)} %all-gather.17.cloned.1.call-done, f32[128,4096]{1,0:T(8,128)} %fusion.15), kind=kOutput, calls=%fused_computation.16 | convolution fusion | flops 1075576832 | bytes 11010048 | tf_op jit(solution)/shard_map/dot_general | solution.py:150
  469.4 13.0 %reduce-scatter.5.cloned.1.call-done = bf16[64,2048]{1,0:T(8,128)(2,1)} async-done(((bf16[128,2048]{1,0:T(8,128)(2,1)}), bf16[64,2048]{1,0:T(8,128)(2,1)}) %reduce-scatter.5.cloned.1.call-update) | async-done | bytes 262160 | tf_op jit(solution)/shard_map/reduce_scatter | solution.py:149
  (190 shorter events, 52.4 us)
Async XLA Ops:
  6.5 207.1 %copy-start = (bf16[512,2048]{1,0:T(8,128)(2,1)S(1)}, bf16[512,2048]{1,0:T(8,128)(2,1)}, u32[]{:S(2)}) copy-start(bf16[512,2048]{1,0:T(8,128)(2,1)} %param.26) | copy-start | bytes 6291460
  6.5 114.3 %copy-start.38 = (f32[128,4]{0,1:T(4,128)S(1)}, f32[128,4]{0,1:T(4,128)}, u32[]{:S(2)}) copy-start(f32[128,4]{0,1:T(4,128)} %param.25) | copy-start | bytes 6148
  6.5 180.6 %all-gather.7.cloned.1.call-start = ((), (), s32[]{:S(2)}) async-start(), calls=%async_computation.2 | async-start | bytes 2228224 | tf_op jit(solution)/shard_map/all_gather | solution.py:107
  7.3 183.8 %all-gather.9.cloned.1.call-start = ((), (), s32[]{:S(2)}) async-start(), calls=%async_computation.3 | async-start | bytes 2228224 | tf_op jit(solution)/shard_map/all_gather | solution.py:114
  9.0 196.7 %all-gather.11.cloned.1.call-start = ((), (), s32[]{:S(2)}) async-start(), calls=%async_computation.4 | async-start | bytes 2228224 | tf_op jit(solution)/shard_map/all_gather | solution.py:115
  9.0 8.4 %collective-permute-start = (bf16[128,512]{1,0:T(8,128)(2,1)}, bf16[128,512]{1,0:T(8,128)(2,1)S(1)}, u32[]{:S(2)}, u32[]{:S(2)}) collective-permute-start(bf16[128,512]{1,0:T(8,128)(2,1)} %param.20), channel_id=1, source_target_pairs={{0,2},{2,4},{4,6},{6,8},{8,10},{10,12},{12,14},{14,16},{16,18},{18... | collective-permute-start | bytes 393224 | tf_op jit(solution)/shard_map/ppermute | solution.py:110
  18.1 7.2 %collective-permute-start.1 = (bf16[128,512]{1,0:T(8,128)(2,1)S(1)}, bf16[128,512]{1,0:T(8,128)(2,1)S(1)}, u32[]{:S(2)}, u32[]{:S(2)}) collective-permute-start(bf16[128,512]{1,0:T(8,128)(2,1)S(1)} %collective-permute-done), channel_id=1, source_target_pairs={{0,2},{2,4},{4,6},{6,8},{8,10},{10,12},{12,14},{14,16},{16,18},{18... | collective-permute-start | bytes 393224 | tf_op jit(solution)/shard_map/ppermute | solution.py:110
  26.0 7.4 %collective-permute-start.2 = (bf16[128,512]{1,0:T(8,128)(2,1)S(1)}, bf16[128,512]{1,0:T(8,128)(2,1)S(1)}, u32[]{:S(2)}, u32[]{:S(2)}) collective-permute-start(bf16[128,512]{1,0:T(8,128)(2,1)S(1)} %collective-permute-done.1), channel_id=1, source_target_pairs={{0,2},{2,4},{4,6},{6,8},{8,10},{10,12},{12,14},{14,16},{16,18},{18... | collective-permute-start | bytes 393224 | tf_op jit(solution)/shard_map/ppermute | solution.py:110
  34.0 7.2 %collective-permute-start.3 = (bf16[128,512]{1,0:T(8,128)(2,1)S(1)}, bf16[128,512]{1,0:T(8,128)(2,1)S(1)}, u32[]{:S(2)}, u32[]{:S(2)}) collective-permute-start(bf16[128,512]{1,0:T(8,128)(2,1)S(1)} %collective-permute-done.2), channel_id=1, source_target_pairs={{0,2},{2,4},{4,6},{6,8},{8,10},{10,12},{12,14},{14,16},{16,18},{18... | collective-permute-start | bytes 393224 | tf_op jit(solution)/shard_map/ppermute | solution.py:110
  41.9 7.9 %collective-permute-start.4 = (bf16[128,512]{1,0:T(8,128)(2,1)S(1)}, bf16[128,512]{1,0:T(8,128)(2,1)S(1)}, u32[]{:S(2)}, u32[]{:S(2)}) collective-permute-start(bf16[128,512]{1,0:T(8,128)(2,1)S(1)} %collective-permute-done.3), channel_id=1, source_target_pairs={{0,2},{2,4},{4,6},{6,8},{8,10},{10,12},{12,14},{14,16},{16,18},{18... | collective-permute-start | bytes 393224 | tf_op jit(solution)/shard_map/ppermute | solution.py:110
  50.4 7.1 %collective-permute-start.5 = (bf16[128,512]{1,0:T(8,128)(2,1)S(1)}, bf16[128,512]{1,0:T(8,128)(2,1)S(1)}, u32[]{:S(2)}, u32[]{:S(2)}) collective-permute-start(bf16[128,512]{1,0:T(8,128)(2,1)S(1)} %collective-permute-done.4), channel_id=1, source_target_pairs={{0,2},{2,4},{4,6},{6,8},{8,10},{10,12},{12,14},{14,16},{16,18},{18... | collective-permute-start | bytes 393224 | tf_op jit(solution)/shard_map/ppermute | solution.py:110
  58.1 7.1 %collective-permute-start.6 = (bf16[128,512]{1,0:T(8,128)(2,1)S(1)}, bf16[128,512]{1,0:T(8,128)(2,1)S(1)}, u32[]{:S(2)}, u32[]{:S(2)}) collective-permute-start(bf16[128,512]{1,0:T(8,128)(2,1)S(1)} %collective-permute-done.5), channel_id=1, source_target_pairs={{0,2},{2,4},{4,6},{6,8},{8,10},{10,12},{12,14},{14,16},{16,18},{18... | collective-permute-start | bytes 393224 | tf_op jit(solution)/shard_map/ppermute | solution.py:110
  65.9 7.2 %collective-permute-start.7 = (bf16[128,512]{1,0:T(8,128)(2,1)S(1)}, bf16[128,512]{1,0:T(8,128)(2,1)S(1)}, u32[]{:S(2)}, u32[]{:S(2)}) collective-permute-start(bf16[128,512]{1,0:T(8,128)(2,1)S(1)} %collective-permute-done.6), channel_id=1, source_target_pairs={{0,2},{2,4},{4,6},{6,8},{8,10},{10,12},{12,14},{14,16},{16,18},{18... | collective-permute-start | bytes 393224 | tf_op jit(solution)/shard_map/ppermute | solution.py:110
  73.1 39.5 %copy-start.24 = (bf16[128,512]{1,0:T(8,128)(2,1)}, bf16[128,512]{1,0:T(8,128)(2,1)S(1)}, u32[]{:S(2)}) copy-start(bf16[128,512]{1,0:T(8,128)(2,1)S(1)} %collective-permute-done.7) | copy-start | bytes 393220
  73.1 7.1 %collective-permute-start.8 = (bf16[128,512]{1,0:T(8,128)(2,1)S(1)}, bf16[128,512]{1,0:T(8,128)(2,1)S(1)}, u32[]{:S(2)}, u32[]{:S(2)}) collective-permute-start(bf16[128,512]{1,0:T(8,128)(2,1)S(1)} %collective-permute-done.7), channel_id=1, source_target_pairs={{0,2},{2,4},{4,6},{6,8},{8,10},{10,12},{12,14},{14,16},{16,18},{18... | collective-permute-start | bytes 393224 | tf_op jit(solution)/shard_map/ppermute | solution.py:110
  73.1 160.2 %reduce-scatter.3.cloned.1.call-start = ((), (), s32[]{:S(2)}) async-start(), calls=%async_computation.5 | async-start | bytes 786432 | tf_op jit(solution)/shard_map/reduce_scatter | solution.py:121
  80.2 32.4 %copy-start.26 = (bf16[128,512]{1,0:T(8,128)(2,1)}, bf16[128,512]{1,0:T(8,128)(2,1)S(1)}, u32[]{:S(2)}) copy-start(bf16[128,512]{1,0:T(8,128)(2,1)S(1)} %collective-permute-done.8) | copy-start | bytes 393220
  80.2 7.3 %collective-permute-start.9 = (bf16[128,512]{1,0:T(8,128)(2,1)S(1)}, bf16[128,512]{1,0:T(8,128)(2,1)S(1)}, u32[]{:S(2)}, u32[]{:S(2)}) collective-permute-start(bf16[128,512]{1,0:T(8,128)(2,1)S(1)} %collective-permute-done.8), channel_id=1, source_target_pairs={{0,2},{2,4},{4,6},{6,8},{8,10},{10,12},{12,14},{14,16},{16,18},{18... | collective-permute-start | bytes 393224 | tf_op jit(solution)/shard_map/ppermute | solution.py:110
  87.5 25.1 %copy-start.28 = (bf16[128,512]{1,0:T(8,128)(2,1)}, bf16[128,512]{1,0:T(8,128)(2,1)S(1)}, u32[]{:S(2)}) copy-start(bf16[128,512]{1,0:T(8,128)(2,1)S(1)} %collective-permute-done.9) | copy-start | bytes 393220
  87.5 24.7 %collective-permute-start.10 = (bf16[128,512]{1,0:T(8,128)(2,1)S(1)}, bf16[128,512]{1,0:T(8,128)(2,1)S(1)}, u32[]{:S(2)}, u32[]{:S(2)}) collective-permute-start(bf16[128,512]{1,0:T(8,128)(2,1)S(1)} %collective-permute-done.9), channel_id=1, source_target_pairs={{0,2},{2,4},{4,6},{6,8},{8,10},{10,12},{12,14},{14,16},{16,18},{18... | collective-permute-start | bytes 393224 | tf_op jit(solution)/shard_map/ppermute | solution.py:110
  112.2 44.9 %copy-start.30 = (bf16[128,512]{1,0:T(8,128)(2,1)}, bf16[128,512]{1,0:T(8,128)(2,1)S(1)}, u32[]{:S(2)}) copy-start(bf16[128,512]{1,0:T(8,128)(2,1)S(1)} %collective-permute-done.10) | copy-start | bytes 393220
  112.2 8.6 %collective-permute-start.11 = (bf16[128,512]{1,0:T(8,128)(2,1)S(1)}, bf16[128,512]{1,0:T(8,128)(2,1)}, u32[]{:S(2)}, u32[]{:S(2)}) collective-permute-start(bf16[128,512]{1,0:T(8,128)(2,1)S(1)} %collective-permute-done.10), channel_id=1, source_target_pairs={{0,2},{2,4},{4,6},{6,8},{8,10},{10,12},{12,14},{14,16},{16,18},{18... | collective-permute-start | bytes 393224 | tf_op jit(solution)/shard_map/ppermute | solution.py:110
  120.8 27.4 %collective-permute-start.12 = (bf16[128,512]{1,0:T(8,128)(2,1)}, bf16[128,512]{1,0:T(8,128)(2,1)}, u32[]{:S(2)}, u32[]{:S(2)}) collective-permute-start(bf16[128,512]{1,0:T(8,128)(2,1)} %collective-permute-done.11), channel_id=1, source_target_pairs={{0,2},{2,4},{4,6},{6,8},{8,10},{10,12},{12,14},{14,16},{16,18},{18... | collective-permute-start | bytes 393224 | tf_op jit(solution)/shard_map/ppermute | solution.py:110
  148.2 7.4 %collective-permute-start.13 = (bf16[128,512]{1,0:T(8,128)(2,1)}, bf16[128,512]{1,0:T(8,128)(2,1)}, u32[]{:S(2)}, u32[]{:S(2)}) collective-permute-start(bf16[128,512]{1,0:T(8,128)(2,1)} %collective-permute-done.12), channel_id=1, source_target_pairs={{0,2},{2,4},{4,6},{6,8},{8,10},{10,12},{12,14},{14,16},{16,18},{18... | collective-permute-start | bytes 393224 | tf_op jit(solution)/shard_map/ppermute | solution.py:110
  155.6 8.0 %collective-permute-start.14 = (bf16[128,512]{1,0:T(8,128)(2,1)}, bf16[128,512]{1,0:T(8,128)(2,1)}, u32[]{:S(2)}, u32[]{:S(2)}) collective-permute-start(bf16[128,512]{1,0:T(8,128)(2,1)} %collective-permute-done.13), channel_id=1, source_target_pairs={{0,2},{2,4},{4,6},{6,8},{8,10},{10,12},{12,14},{14,16},{16,18},{18... | collective-permute-start | bytes 393224 | tf_op jit(solution)/shard_map/ppermute | solution.py:110
  216.5 93.1 %all-gather.15.cloned.1.call-start = ((), (), s32[]{:S(2)}) async-start(), calls=%async_computation.7 | async-start | bytes 8912896 | tf_op jit(solution)/shard_map/all_gather | solution.py:86
  217.1 167.5 %all-gather.13.cloned.1.call-start = ((), (), s32[]{:S(2)}) async-start(), calls=%async_computation.6 | async-start | bytes 8912896 | tf_op jit(solution)/shard_map/all_gather | solution.py:85
  217.7 245.4 %all-gather.17.cloned.1.call-start = ((), (), s32[]{:S(2)}) async-start(), calls=%async_computation.8 | async-start | bytes 8912896 | tf_op jit(solution)/shard_map/all_gather | solution.py:87
  218.4 263.9 %reduce-scatter.5.cloned.1.call-start = ((), (), s32[]{:S(2)}) async-start(), calls=%async_computation.9 | async-start | bytes 786432 | tf_op jit(solution)/shard_map/reduce_scatter | solution.py:149
  389.3 3.0 collective-permute-start.15
  394.5 87.9 %copy-start.5 = (bf16[64,2048]{1,0:T(8,128)(2,1)S(1)}, bf16[64,2048]{1,0:T(8,128)(2,1)}, u32[]{:S(2)}) copy-start(bf16[64,2048]{1,0:T(8,128)(2,1)} %reduce-scatter.3.cloned.1.call-done) | copy-start | bytes 786436
  463.1 21.0 %copy-start.1 = (bf16[512,2048]{1,0:T(8,128)(2,1)S(1)}, bf16[512,2048]{1,0:T(8,128)(2,1)}, u32[]{:S(2)}) copy-start(bf16[512,2048]{1,0:T(8,128)(2,1)} %param.26) | copy-start | bytes 6291460
  (32 other events, 314.1 us)
Sparse Core Ops, SparseCore 0:
  9.5 45.7 all-gather.6
  57.4 42.6 all-gather.8
  102.2 43.4 all-gather.10
  216.6 16.6 reduce-scatter.2
  235.3 74.2 all-gather.14
  311.7 72.8 all-gather.12
  386.7 76.2 all-gather.16
  469.5 12.7 reduce-scatter.4
